TPU v7x, 32 devices: a whole 2x2x4 slice. The times are simulated.
32 devices in a mesh: kv: 8 (over y, x, core), tp: 4 (over z).
Axes of the slice: x: 2, y: 2, z: 4, core: 2. Of those that a mesh axis runs over, the one named last changes fastest.
Arguments:
- tokens: bfloat16 [64, 4, 4096], P(None, None, ('kv', 'tp')), may hold values from -36 to 36
- lengths: int32 [64], replicated, may hold values from 1 to 4, 112 in all
- state: float32 [64, 128, 4096], P('kv', None, 'tp'), may hold values from -0.6 to 0.6
- attn_gain: float32 [4096], P('kv'), may hold values from 0.1 to 1.9
- w_query: bfloat16 [4096, 4096], P('kv', 'tp'), may hold values from -0.09375 to 0.09375
- w_key: bfloat16 [4096, 4096], P('kv', 'tp'), may hold values from -0.09375 to 0.09375
- w_value: bfloat16 [4096, 4096], P('kv', 'tp'), may hold values from -0.09375 to 0.09375
- w_beta: bfloat16 [4096, 32], replicated, may hold values from -0.09375 to 0.09375
- w_alpha: bfloat16 [4096, 32], replicated, may hold values from -0.09375 to 0.09375
- decay_rate: float32 [32], replicated, may hold values from 0.05 to 3
- decay_bias: float32 [32], replicated, may hold values from -3 to 3
- out_gain: float32 [128], replicated, may hold values from 0.1 to 1.9
- w_out: bfloat16 [4096, 4096], P('tp', 'kv'), may hold values from -0.09375 to 0.09375
- mix_gain: float32 [4096], P('kv'), may hold values from 0.1 to 1.9
- w_gate: bfloat16 [4096, 11008], P('kv', 'tp'), may hold values from -0.09375 to 0.09375
- w_up: bfloat16 [4096, 11008], P('kv', 'tp'), may hold values from -0.09375 to 0.09375
- w_down: bfloat16 [11008, 4096], P('tp', 'kv'), may hold values from -0.0546875 to 0.0546875
Outputs:
- mixed: bfloat16 [64, 4, 4096], P(None, None, ('kv', 'tp'))
- new_state: float32 [64, 128, 4096], P('kv', None, 'tp')
Inputs may be any that keep to these rules, and one draw needn't show every extreme that they name: Each sequence has 1 to 4 live tokens, the first ones of its block, and the lengths sum to 112.
All inputs are finite; a program needn't handle non-finite values.
Results may differ from a plain program's by a relative error of at most 0.015.
Values may be sent and summed in bfloat16 or wider, within the bound.
A program may use at most 64 MiB of HBM per device.

v0:
```python
import jax
import jax.numpy as jnp
from jax import lax
from jax.sharding import PartitionSpec as P

D = 4096
HEAD_DIM = 128
EPSILON = 1e-06


def unit_rows(vectors):
    return vectors * lax.rsqrt(jnp.sum(vectors * vectors, axis=-1, keepdims=True) + EPSILON)


def delta_block(queries, unit_keys, values_split, beta, log_decay, carried):
    highest = lax.Precision.HIGHEST
    seq_count, span_len, heads_here = beta.shape
    cumulative = jnp.cumsum(log_decay, axis=1)
    position = jnp.arange(span_len)
    inclusive = (position[:, None] >= position[None, :])[None, :, :, None]
    strict = (position[:, None] > position[None, :])[None, :, :, None]
    gap_matrix = cumulative[:, :, None, :] - cumulative[:, None, :, :]
    decay_matrix = jnp.where(inclusive, jnp.exp(jnp.where(inclusive, gap_matrix, 0.0)), 0.0)
    key_dots = jnp.einsum("nihd,njhd->nijh", unit_keys, unit_keys, precision=highest)
    query_dots = jnp.einsum("nihd,njhd->nijh", queries, unit_keys, precision=highest) * decay_matrix
    lower_part = jnp.where(strict, key_dots * decay_matrix * beta[:, :, None, :], 0.0)
    identity = jnp.eye(span_len, dtype=jnp.float32)
    inverse_rows = []
    for step in range(span_len):
        row_now = jnp.broadcast_to(identity[step][None, :, None], (seq_count, span_len, heads_here))
        for prior in range(step):
            row_now = row_now - lower_part[:, step, prior, :][:, None, :] * inverse_rows[prior]
        inverse_rows.append(row_now)
    inverse = jnp.stack(inverse_rows, axis=1)
    beta_value = beta[..., None] * values_split
    beta_key = (beta * jnp.exp(cumulative))[..., None] * unit_keys
    base_update = jnp.einsum("nich,nche->nihe", inverse, beta_value, precision=highest)
    key_weights = jnp.einsum("nich,nchd->nihd", inverse, beta_key, precision=highest)
    corrected = base_update - jnp.einsum("nihd,ndhe->nihe", key_weights, carried, precision=highest)
    decayed_queries = queries * jnp.exp(cumulative)[..., None]
    attended = jnp.einsum("nihd,ndhe->nihe", decayed_queries, carried, precision=highest)
    attended = attended + jnp.einsum("nijh,njhe->nihe", query_dots, corrected, precision=highest)
    block_total = cumulative[:, -1, :]
    key_tail = unit_keys * jnp.exp(block_total[:, None, :] - cumulative)[..., None]
    updated = carried * jnp.exp(block_total)[:, None, :, None]
    updated = updated + jnp.einsum("nihd,nihe->ndhe", key_tail, corrected, precision=highest)
    return (attended, updated)


def body(
    tokens,
    lengths,
    state,
    attn_gain,
    w_query,
    w_key,
    w_value,
    w_beta,
    w_alpha,
    decay_rate,
    decay_bias,
    out_gain,
    w_out,
    mix_gain,
    w_gate,
    w_up,
    w_down,
):
    kv_index = lax.axis_index("kv")
    tp_index = lax.axis_index("tp")
    kv_count = lax.axis_size("kv")
    batch_all, span_len, own_cols = tokens.shape
    row_count = batch_all * span_len
    seq_count = state.shape[0]
    local_rows = seq_count * span_len
    head_size = state.shape[1]
    heads_here = state.shape[2] // head_size
    block_width = attn_gain.shape[0]
    flat_rows = tokens.reshape(row_count, own_cols)
    live_all = (jnp.arange(span_len, dtype=jnp.int32)[None, :] < lengths[:, None]).reshape(
        row_count, 1
    )
    gathered = lax.all_gather(flat_rows, "tp", axis=1, tiled=True).astype(jnp.float32)
    squares_in = jnp.sum(gathered * gathered, axis=1)
    normed_in = (gathered * attn_gain).astype(jnp.bfloat16)
    beta_rows = lax.dynamic_slice_in_dim(w_beta, kv_index * block_width, block_width, 0)
    alpha_rows = lax.dynamic_slice_in_dim(w_alpha, kv_index * block_width, block_width, 0)
    query_part = jnp.dot(normed_in, w_query, preferred_element_type=jnp.float32)
    key_part = jnp.dot(normed_in, w_key, preferred_element_type=jnp.float32)
    value_part = jnp.dot(normed_in, w_value, preferred_element_type=jnp.float32)
    beta_part = jnp.dot(normed_in, beta_rows, preferred_element_type=jnp.float32)
    alpha_part = jnp.dot(normed_in, alpha_rows, preferred_element_type=jnp.float32)
    squares_all = lax.psum(squares_in, "kv")
    squares_own = lax.dynamic_slice_in_dim(squares_all, kv_index * local_rows, local_rows, 0)
    query_sum, key_sum, value_sum, beta_sum, alpha_sum = (
        lax.psum_scatter(
            query_part.astype(jnp.bfloat16), "kv", scatter_dimension=0, tiled=True
        ).astype(jnp.float32),
        lax.psum_scatter(
            key_part.astype(jnp.bfloat16), "kv", scatter_dimension=0, tiled=True
        ).astype(jnp.float32),
        lax.psum_scatter(
            value_part.astype(jnp.bfloat16), "kv", scatter_dimension=0, tiled=True
        ).astype(jnp.float32),
        lax.psum_scatter(
            beta_part.astype(jnp.bfloat16), "kv", scatter_dimension=0, tiled=True
        ).astype(jnp.float32),
        lax.psum_scatter(
            alpha_part.astype(jnp.bfloat16), "kv", scatter_dimension=0, tiled=True
        ).astype(jnp.float32),
    )
    row_scale = lax.rsqrt(squares_own / D + EPSILON)[:, None]
    head_start = tp_index * heads_here
    lengths_own = lax.dynamic_slice_in_dim(lengths, kv_index * seq_count, seq_count, 0)
    live_own = (jnp.arange(span_len, dtype=jnp.int32)[None, :] < lengths_own[:, None])[..., None]
    beta_heads = lax.dynamic_slice_in_dim(beta_sum, head_start, heads_here, 1) * row_scale
    alpha_heads = lax.dynamic_slice_in_dim(alpha_sum, head_start, heads_here, 1) * row_scale
    rate_here = lax.dynamic_slice_in_dim(decay_rate, head_start, heads_here, 0)
    bias_here = lax.dynamic_slice_in_dim(decay_bias, head_start, heads_here, 0)
    beta = jnp.where(
        live_own, jax.nn.sigmoid(beta_heads).reshape(seq_count, span_len, heads_here), 0.0
    )
    log_decay = -rate_here * jax.nn.softplus(alpha_heads + bias_here)
    log_decay = jnp.where(live_own, log_decay.reshape(seq_count, span_len, heads_here), 0.0)
    split_shape = (seq_count, span_len, heads_here, head_size)
    queries = unit_rows((query_sum * row_scale).reshape(split_shape)) * HEAD_DIM ** (-0.5)
    unit_keys = unit_rows((key_sum * row_scale).reshape(split_shape))
    values_split = (value_sum * row_scale).reshape(split_shape)
    carried = state.reshape(seq_count, head_size, heads_here, head_size)
    attended, updated = delta_block(queries, unit_keys, values_split, beta, log_decay, carried)
    head_out = (
        attended
        * lax.rsqrt(jnp.mean(attended * attended, axis=-1, keepdims=True) + EPSILON)
        * out_gain
    )
    head_out = head_out.astype(jnp.bfloat16).reshape(local_rows, heads_here * head_size)
    pack_rows = min((batch_all * 7 // 4 + kv_count - 1) // kv_count * kv_count, row_count)
    live_flat = live_all.reshape(row_count).astype(jnp.int32)
    slot_index = jnp.cumsum(live_flat) - 1
    picker = (
        (slot_index[None, :] == jnp.arange(pack_rows, dtype=jnp.int32)[:, None])
        & (live_flat[None, :] > 0)
    ).astype(jnp.bfloat16)
    heads_every = lax.all_gather(head_out, "kv", axis=0, tiled=True)
    packed_heads = jnp.dot(picker, heads_every, preferred_element_type=jnp.float32).astype(
        jnp.bfloat16
    )
    attn_part = jnp.dot(packed_heads, w_out, preferred_element_type=jnp.float32)
    base_rows = jnp.dot(picker, flat_rows, preferred_element_type=jnp.float32)
    attn_own = lax.psum_scatter(
        attn_part.astype(jnp.bfloat16), "tp", scatter_dimension=1, tiled=True
    ).astype(jnp.float32)
    middle = (base_rows + attn_own).astype(jnp.bfloat16)
    middle_rows = lax.all_gather(middle, "tp", axis=1, tiled=True).astype(jnp.float32)
    squares_mid = jnp.sum(middle_rows * middle_rows, axis=1)
    normed_mid = (middle_rows * mix_gain).astype(jnp.bfloat16)
    gate_part = jnp.dot(normed_mid, w_gate, preferred_element_type=jnp.float32)
    up_part = jnp.dot(normed_mid, w_up, preferred_element_type=jnp.float32)
    squares_total = lax.psum(squares_mid, "kv")
    gate_sum, up_sum = (
        lax.psum(gate_part.astype(jnp.bfloat16), "kv").astype(jnp.float32),
        lax.psum(up_part.astype(jnp.bfloat16), "kv").astype(jnp.float32),
    )
    mid_scale = lax.rsqrt(squares_total / D + EPSILON)[:, None]
    hidden = (jax.nn.silu(gate_sum * mid_scale) * (up_sum * mid_scale)).astype(jnp.bfloat16)
    down_part = jnp.dot(hidden, w_down, preferred_element_type=jnp.float32)
    down_own = lax.psum_scatter(
        down_part.astype(jnp.bfloat16), "tp", scatter_dimension=1, tiled=True
    ).astype(jnp.float32)
    result_rows = middle.astype(jnp.float32) + down_own
    result_rows = jnp.dot(
        picker.astype(jnp.float32).T,
        result_rows,
        precision=lax.Precision.HIGHEST,
        preferred_element_type=jnp.float32,
    )
    mixed = (
        jnp.where(live_all, result_rows, 0.0)
        .astype(jnp.bfloat16)
        .reshape(batch_all, span_len, own_cols)
    )
    return (mixed, updated.reshape(seq_count, head_size, heads_here * head_size))


def solution(mesh):
    return jax.shard_map(
        body,
        mesh=mesh,
        in_specs=(
            P(None, None, ("kv", "tp")),
            P(),
            P("kv", None, "tp"),
            P("kv"),
            P("kv", "tp"),
            P("kv", "tp"),
            P("kv", "tp"),
            P(),
            P(),
            P(),
            P(),
            P(),
            P("tp", "kv"),
            P("kv"),
            P("kv", "tp"),
            P("kv", "tp"),
            P("tp", "kv"),
        ),
        out_specs=(P(None, None, ("kv", "tp")), P("kv", None, "tp")),
        check_vma=False,
    )
```

profile of v0, /device:TPU:0, one launch (start us, length us, event | category | flops | bytes accessed | tf_op | source)
XLA Modules:
  0.0 369.6 jit_solution(18087534690063010372)
XLA Ops:
  7.2 14.8 %all_gather.9 = bf16[256,512]{1,0:T(8,128)(2,1)S(1)} all-gather(bf16[256,128]{1,0:T(8,128)(2,1)} %bitcast.99), channel_id=1, replica_groups=mesh['kv'=8,'tp'=4] {'tp'}, dimensions={1}, use_global_device_ids=true | all-gather | bytes 327680 | tf_op jit(solution)/shard_map/all_gather | solution.py:83
  22.1 1.6 convolution_convert_fusion.7
  23.8 1.6 convolution_convert_fusion.8
  25.5 2.5 convolution_convert_fusion.4
  28.0 2.5 convolution_convert_fusion.3
  30.6 2.5 convolution_convert_fusion.2
  33.1 0.1 fusion.13
  33.6 12.2 %psum.28 = f32[256]{0:T(256)S(1)} all-reduce(f32[256]{0:T(256)S(1)} %fusion.13), channel_id=1, replica_groups=mesh['kv'=8,'tp'=4] {'kv'}, use_global_device_ids=true, to_apply=%region_4.0 | all-reduce | flops 256 | bytes 2048 | tf_op jit(solution)/shard_map/psum | solution.py:93
  46.1 5.3 %copy.107 = f32[8,128,1024]{1,2,0:T(8,128)} copy(f32[8,128,1024]{2,1,0:T(8,128)} %param.19) | data formatting | bytes 8388608 | tf_op args[2]
  51.7 0.3 reduce-window.9
  52.2 0.7 add_bitcast_fusion
  52.9 0.5 convert_compare_fusion
  53.5 4.4 %reduce-scatter.16.cloned.1.call-done = bf16[32,32]{1,0:T(8,128)(2,1)} async-done(((bf16[256,32]{1,0:T(8,128)(2,1)}), bf16[32,32]{1,0:T(8,128)(2,1)}) %reduce-scatter.16.cloned.1.call-update) | async-done | bytes 2064 | tf_op jit(solution)/shard_map/reduce_scatter | solution.py:105
  57.9 36.5 %reduce-scatter.14.cloned.1.call-done = bf16[32,32]{1,0:T(8,128)(2,1)} async-done(((bf16[256,32]{1,0:T(8,128)(2,1)}), bf16[32,32]{1,0:T(8,128)(2,1)}) %reduce-scatter.14.cloned.1.call-update) | async-done | bytes 2064 | tf_op jit(solution)/shard_map/reduce_scatter | solution.py:108
  94.4 0.8 add_divide_fusion
  95.6 36.0 %reduce-scatter.12.cloned.1.call-done = bf16[32,1024]{1,0:T(8,128)(2,1)} async-done(((bf16[256,1024]{1,0:T(8,128)(2,1)}), bf16[32,1024]{1,0:T(8,128)(2,1)}) %reduce-scatter.12.cloned.1.call-update) | async-done | bytes 65552 | tf_op jit(solution)/shard_map/reduce_scatter | solution.py:96
  131.6 37.1 %reduce-scatter.18.cloned.1.call-done = bf16[32,1024]{1,0:T(8,128)(2,1)} async-done(((bf16[256,1024]{1,0:T(8,128)(2,1)}), bf16[32,1024]{1,0:T(8,128)(2,1)}) %reduce-scatter.18.cloned.1.call-update) | async-done | bytes 65552 | tf_op jit(solution)/shard_map/reduce_scatter | solution.py:102
  168.7 37.1 %reduce-scatter.20.cloned.1.call-done = bf16[32,1024]{1,0:T(8,128)(2,1)} async-done(((bf16[256,1024]{1,0:T(8,128)(2,1)}), bf16[32,1024]{1,0:T(8,128)(2,1)}) %reduce-scatter.20.cloned.1.call-update) | async-done | bytes 65552 | tf_op jit(solution)/shard_map/reduce_scatter | solution.py:99
  205.8 1.0 multiply_bitcast_fusion.2
  207.2 0.9 multiply_multiply_fusion.1
  208.1 0.6 fusion.6
  208.6 1.1 slice_reduce_fusion.4
  209.9 0.3 copy.120
  210.3 1.4 convolution_bitcast_fusion.5
  211.7 0.6 convolution_bitcast_fusion.4
  212.2 1.6 fusion.7
  213.9 8.6 %fusion.2 = f32[8,4,8,128]{3,1,2,0:T(4,128)S(1)} fusion(f32[8,4,8,128]{3,1,2,0:T(4,128)S(1)} %convolution_bitcast_fusion.5, f32[8,4,8,128]{3,1,2,0:T(4,128)S(1)} %convolution_bitcast_fusion.4, f32[8,128,8,128]{1,3,2,0:T(8,128)} %bitcast.86), kind=kOutput, calls=%fused_computation.12 | convolution fusion | flops 50364416 | bytes 4587520 | tf_op jit(solution)/shard_map/nihd,ndhe->nihe/dot_general | solution.py:39
  222.5 0.7 convolution_bitcast_fusion.2
  223.2 6.7 %multiply_reduce_fusion = (f32[8,4,8]{1,2,0:T(8,128)S(1)}, f32[8,4,8,128]{3,1,2,0:T(4,128)S(1)}) fusion(f32[8,4,8,128]{3,1,2,0:T(4,128)S(1)} %convolution_bitcast_fusion.2, f32[8,128,8,128]{1,3,2,0:T(8,128)S(1)} %bitcast.88, f32[8,4,8,128]{3,2,1,0:T(8,128)S(1)} %get-tuple-element.24), kind=kOutput, calls=%fused_computation.46 | convolution fusion | flops 50429696 | bytes 4588544 | tf_op jit(solution)/shard_map/nihd,ndhe->nihe/dot_general | solution.py:41
  230.1 0.1 multiply_convert_fusion.2
  230.3 9.8 %all_gather.10 = bf16[256,1024]{1,0:T(8,128)(2,1)S(1)} all-gather(bf16[32,1024]{1,0:T(8,128)(2,1)S(1)} %bitcast.96), channel_id=1, replica_groups=mesh['kv'=8,'tp'=4] {'kv'}, dimensions={0}, use_global_device_ids=true | all-gather | bytes 589824 | tf_op jit(solution)/shard_map/all_gather | solution.py:144
  240.1 2.3 fusion.1
  242.4 1.7 copy.137
  244.2 19.5 %reduce-scatter.22.cloned.1.call-done = bf16[128,112]{1,0:T(8,128)(2,1)} async-done(((bf16[512,112]{1,0:T(8,128)(2,1)}), bf16[128,112]{1,0:T(8,128)(2,1)}) %reduce-scatter.22.cloned.1.call-update) | async-done | bytes 28688
  263.7 0.9 copy.138
  264.6 1.0 fusion.9
  265.5 12.2 %all_gather.11 = bf16[112,512]{1,0:T(8,128)(2,1)S(1)} all-gather(bf16[112,128]{1,0:T(8,128)(2,1)S(1)} %fusion.9), channel_id=1, replica_groups=mesh['kv'=8,'tp'=4] {'tp'}, dimensions={1}, use_global_device_ids=true | all-gather | bytes 143360 | tf_op jit(solution)/shard_map/all_gather | solution.py:154
  277.7 2.6 convolution_convert_fusion
  280.3 1.8 convolution_convert_fusion.1
  282.3 12.1 %psum.30 = f32[112]{0:T(128)S(1)} all-reduce(f32[112]{0:T(128)S(1)} %fusion.15), channel_id=1, replica_groups=mesh['kv'=8,'tp'=4] {'kv'}, use_global_device_ids=true, to_apply=%region_16.17 | all-reduce | flops 112 | bytes 896 | tf_op jit(solution)/shard_map/psum | solution.py:159
  294.5 44.0 %all-reduce.3.cloned.1.call-done = (bf16[112,2752]{1,0:T(8,128)(2,1)}, bf16[112,2752]{1,0:T(8,128)(2,1)}) async-done(((bf16[112,2752]{1,0:T(8,128)(2,1)}, bf16[112,2752]{1,0:T(8,128)(2,1)}), (bf16[112,2752]{1,0:T(8,128)(2,1)}, bf16[112,2752]{1,0:T(8,128)(2,1)})) %all-reduce.3.cloned.1.call-update) | async-done | bytes 1232912 | tf_op jit(solution)/shard_map/psum | solution.py:162
  338.5 2.9 convolution_convert_fusion.6
  341.4 0.7 copy.139
  342.2 10.2 %bitcast_add_fusion = f32[8,128,8,128]{1,3,2,0:T(8,128)} fusion(f32[8,128,8,128]{1,3,2,0:T(8,128)} %bitcast.87, f32[8,4,8,128]{3,1,2,0:T(4,128)S(1)} %fusion.2, f32[8,8]{1,0:T(8,128)S(1)} %fusion.59, f32[8,4,8,128]{3,2,1,0:T(8,128)S(1)} %copy-done.3), kind=kOutput, calls=%fused_computation | convolution fusion | flops 52428800 | bytes 8651008 | tf_op jit(solution)/shard_map/nihd,nihe->ndhe/dot_general | solution.py:46
  352.4 5.4 %copy.133 = f32[8,128,1024]{2,1,0:T(8,128)} copy(f32[8,128,1024]{1,2,0:T(8,128)} %bitcast.89) | data formatting | bytes 8388608
  357.8 3.2 reduce-scatter.24.cloned.1.call-done
  360.9 0.9 copy.140
  361.8 0.9 fusion.8
  (96 shorter events, 3.1 us)
Async XLA Ops:
  7.2 270.6 %copy-start = (bf16[512,2752]{0,1:T(8,128)(2,1)S(1)}, bf16[512,2752]{0,1:T(8,128)(2,1)}, u32[]{:S(2)}) copy-start(bf16[512,2752]{0,1:T(8,128)(2,1)} %param.32) | copy-start | bytes 8454148
  7.2 20.8 %copy-start.6 = (f32[512]{0:T(512)S(1)}, f32[512]{0:T(512)}, u32[]{:S(2)}) copy-start(f32[512]{0:T(512)} %param.20) | copy-start | bytes 6148
  7.2 50.7 %reduce-scatter.16.cloned.1.call-start = ((), (), s32[]{:S(2)}) async-start(), calls=%async_computation.9 | async-start | bytes 73728 | tf_op jit(solution)/shard_map/reduce_scatter | solution.py:105
  23.7 70.7 %reduce-scatter.14.cloned.1.call-start = ((), (), s32[]{:S(2)}) async-start(), calls=%async_computation.8 | async-start | bytes 73728 | tf_op jit(solution)/shard_map/reduce_scatter | solution.py:108
  25.4 106.2 %reduce-scatter.12.cloned.1.call-start = ((), (), s32[]{:S(2)}) async-start(), calls=%async_computation.7 | async-start | bytes 589824 | tf_op jit(solution)/shard_map/reduce_scatter | solution.py:96
  27.9 5.4 %copy-start.11 = (s32[64]{0:T(128)S(1)}, s32[64]{0:T(128)}, u32[]{:S(2)}) copy-start(s32[64]{0:T(128)} %param.18) | copy-start | bytes 772
  27.9 17.9 %copy-start.14 = (f32[32]{0:T(128)S(1)}, f32[32]{0:T(128)}, u32[]{:S(2)}) copy-start(f32[32]{0:T(128)} %param.27) | copy-start | bytes 388
  27.9 18.0 %copy-start.15 = (f32[32]{0:T(128)S(1)}, f32[32]{0:T(128)}, u32[]{:S(2)}) copy-start(f32[32]{0:T(128)} %param.26) | copy-start | bytes 388
  28.0 140.8 %reduce-scatter.18.cloned.1.call-start = ((), (), s32[]{:S(2)}) async-start(), calls=%async_computation.10 | async-start | bytes 589824 | tf_op jit(solution)/shard_map/reduce_scatter | solution.py:102
  30.5 175.3 %reduce-scatter.20.cloned.1.call-start = ((), (), s32[]{:S(2)}) async-start(), calls=%async_computation.11 | async-start | bytes 589824 | tf_op jit(solution)/shard_map/reduce_scatter | solution.py:99
  33.1 230.6 %reduce-scatter.22.cloned.1.call-start = ((), (), s32[]{:S(2)}) async-start(), calls=%async_computation.12 | async-start | bytes 163840
  33.6 19.3 %copy-start.12 = (pred[256]{0:T(512)(128)(4,1)}, pred[256]{0:T(512)(128)(4,1)S(1)}, u32[]{:S(2)}) copy-start(pred[256]{0:T(512)(128)(4,1)S(1)} %lt.76) | copy-start | bytes 772
  95.6 114.2 %copy-start.5 = (f32[8,4,8]{1,2,0:T(8,128)}, f32[8,4,8]{1,2,0:T(8,128)S(1)}, u32[]{:S(2)}) copy-start(f32[8,4,8]{1,2,0:T(8,128)S(1)} %copy.111) | copy-start | bytes 3076
  212.2 10.9 %copy-start.1 = (f32[8,128,1024]{1,2,0:T(8,128)S(1)}, f32[8,128,1024]{1,2,0:T(8,128)}, u32[]{:S(2)}) copy-start(f32[8,128,1024]{1,2,0:T(8,128)} %copy.107) | copy-start | bytes 12582916
  222.5 7.7 %copy-start.9 = (f32[128]{0:T(128)S(1)}, f32[128]{0:T(128)}, u32[]{:S(2)}) copy-start(f32[128]{0:T(128)} %param.28) | copy-start | bytes 1540
  229.9 34.7 %copy-start.4 = (bf16[64,4,128]{2,1,0:T(4,128)(2,1)S(1)}, bf16[64,4,128]{2,1,0:T(4,128)(2,1)}, u32[]{:S(2)}) copy-start(bf16[64,4,128]{2,1,0:T(4,128)(2,1)} %param.17) | copy-start | bytes 196612
  242.4 37.9 %copy-start.7 = (f32[512]{0:T(512)S(1)}, f32[512]{0:T(512)}, u32[]{:S(2)}) copy-start(f32[512]{0:T(512)} %param.30) | copy-start | bytes 6148
  244.1 94.4 %all-reduce.3.cloned.1.call-start = ((), (), s32[]{:S(2)}) async-start(), calls=%async_computation.14 | async-start | bytes 2523136 | tf_op jit(solution)/shard_map/psum | solution.py:162
  264.6 15.7 %copy-start.2 = (bf16[512,2752]{0,1:T(8,128)(2,1)S(1)}, bf16[512,2752]{0,1:T(8,128)(2,1)}, u32[]{:S(2)}) copy-start(bf16[512,2752]{0,1:T(8,128)(2,1)} %param.31) | copy-start | bytes 8454148
  282.2 78.8 %reduce-scatter.24.cloned.1.call-start = ((), (), s32[]{:S(2)}) async-start(), calls=%async_computation.13 | async-start | bytes 163840
  338.5 3.7 copy-start.3
  352.4 9.4 %copy-start.8 = (s32[256]{0:T(256)S(1)}, s32[256]{0:T(256)}, u32[]{:S(2)}) copy-start(s32[256]{0:T(256)} %add_bitcast_fusion) | copy-start | bytes 3076
  352.4 9.4 %copy-start.10 = (pred[256]{0:T(512)(128)(4,1)S(1)}, pred[256]{0:T(512)(128)(4,1)}, u32[]{:S(2)}) copy-start(pred[256]{0:T(512)(128)(4,1)} %convert_compare_fusion) | copy-start | bytes 772
  352.4 9.4 %copy-start.13 = (pred[256]{0:T(512)(128)(4,1)S(1)}, pred[256]{0:T(512)(128)(4,1)}, u32[]{:S(2)}) copy-start(pred[256]{0:T(512)(128)(4,1)} %copy-done.12) | copy-start | bytes 772
Sparse Core Ops, SparseCore 0:
  23.8 34.0 reduce-scatter.15
  60.9 33.4 reduce-scatter.13
  97.5 34.1 reduce-scatter.11
  134.6 34.1 reduce-scatter.17
  171.6 34.1 reduce-scatter.19
  244.2 19.4 reduce-scatter.21
  282.3 56.1 all-reduce.2
  342.3 18.6 reduce-scatter.23
where the time goes:
time: 371 us; the launch traced here: 370 us
  waiting for transfers between devices  218 us (59%)
  blocking collectives  61.2 us (16%)
  matrix products  52.5 us (14%)
  local copies, waits for them, and re-layouts  17.7 us (5%)
  between operations  14.5 us (4%)
  other arithmetic  5.46 us (1%)
    psum x1, waiting for transfers between devices, body(): lax.psum(up_part.astype(jnp.bfloat16), 'kv').astype(jnp.float32)  44 us
    reduce_scatter x1, waiting for transfers between devices, body(): lax.psum_scatter(value_part.astype(jnp.bfloat16), 'kv', scatter_dimension...  37.1 us
    reduce_scatter x1, waiting for transfers between devices, body(): lax.psum_scatter(key_part.astype(jnp.bfloat16), 'kv', scatter_dimension=0...  37.1 us
    reduce_scatter x1, waiting for transfers between devices, body(): lax.psum_scatter(alpha_part.astype(jnp.bfloat16), 'kv', scatter_dimension...  36.5 us
    reduce_scatter x1, waiting for transfers between devices, body(): lax.psum_scatter(query_part.astype(jnp.bfloat16), 'kv', scatter_dimension...  36 us
    unnamed x10, waiting for transfers between devices  22.8 us
    unnamed x42, local copies, waits for them, and re-layouts  15 us
    all_gather x1, blocking collectives, body(): lax.all_gather(flat_rows, 'tp', axis=1, tiled=True).astype(jnp.float32)  14.8 us
  transfers between devices with their start and end apart: 8, of which 8 were waited for; matrix products, arithmetic and copies ran while one was open for 9% of the time, Pallas kernels for 0%

commit v1 on v0

--- a/solution.py
+++ b/solution.py
@@ -157,9 +157,14 @@
     gate_part = jnp.dot(normed_mid, w_gate, preferred_element_type=jnp.float32)
     up_part = jnp.dot(normed_mid, w_up, preferred_element_type=jnp.float32)
     squares_total = lax.psum(squares_mid, "kv")
+
+    def enter_panel(vector):
+        r_now = lax.all_gather(vector, axis_name="kv").sum(axis=0)
+        return r_now
+
     gate_sum, up_sum = (
         lax.psum(gate_part.astype(jnp.bfloat16), "kv").astype(jnp.float32),
-        lax.psum(up_part.astype(jnp.bfloat16), "kv").astype(jnp.float32),
+        enter_panel(up_part.astype(jnp.bfloat16)).astype(jnp.float32),
     )
     mid_scale = lax.rsqrt(squares_total / D + EPSILON)[:, None]
     hidden = (jax.nn.silu(gate_sum * mid_scale) * (up_sum * mid_scale)).astype(jnp.bfloat16)

time: 371 us -> 410 us (1.11)
  waiting for transfers between devices: 218 us -> 250 us
  other arithmetic: 5.46 us -> 10.2 us
    reduce_scatter x1, waiting for transfers between devices: 36.5 us -> 3.69 us  [body(): lax.psum_scatter(alpha_part.astype(jnp.bfloat16), 'kv', scatter_dimension...]
    reduce_scatter x1, waiting for transfers between devices: 4.39 us -> 37.1 us  [body(): lax.psum_scatter(beta_part.astype(jnp.bfloat16), 'kv', scatter_dimension=...]
    all_gather x0 -> x1, waiting for transfers between devices: none -> 22.3 us  [enter_panel(): r_now = lax.all_gather(vector, axis_name='kv').sum(axis=0)]
    psum x1, waiting for transfers between devices: 44 us -> 54.2 us  [body(): lax.psum(gate_part.astype(jnp.bfloat16), 'kv').astype(jnp.float32)]
    reduce_sum x0 -> x1, other arithmetic: none -> 4.15 us  [enter_panel(): r_now = lax.all_gather(vector, axis_name='kv').sum(axis=0)]
    unnamed x10 -> x11, waiting for transfers between devices: 22.8 us -> 23.1 us
  transfers between devices with their start and end apart: 8 -> 9, of which waited for: 8 -> 9; matrix products, arithmetic and copies ran while one was open for 9% -> 11% of each run, Pallas kernels for 0% -> 0%
where the time goes in v1:
time: 410 us; the launch traced here: 409 us
  waiting for transfers between devices  250 us (61%)
  blocking collectives  61.6 us (15%)
  matrix products  54.3 us (13%)
  local copies, waits for them, and re-layouts  18.3 us (4%)
  between operations  14.2 us (3%)
  other arithmetic  10.2 us (2%)
    psum x1, waiting for transfers between devices, body(): lax.psum(gate_part.astype(jnp.bfloat16), 'kv').astype(jnp.float32)  54.2 us
    reduce_scatter x1, waiting for transfers between devices, body(): lax.psum_scatter(key_part.astype(jnp.bfloat16), 'kv', scatter_dimension=0...  37.1 us
    reduce_scatter x1, waiting for transfers between devices, body(): lax.psum_scatter(beta_part.astype(jnp.bfloat16), 'kv', scatter_dimension=...  37.1 us
    reduce_scatter x1, waiting for transfers between devices, body(): lax.psum_scatter(query_part.astype(jnp.bfloat16), 'kv', scatter_dimension...  37.1 us
    reduce_scatter x1, waiting for transfers between devices, body(): lax.psum_scatter(value_part.astype(jnp.bfloat16), 'kv', scatter_dimension...  35.4 us
    unnamed x11, waiting for transfers between devices  23.1 us
    all_gather x1, waiting for transfers between devices, enter_panel(): r_now = lax.all_gather(vector, axis_name='kv').sum(axis=0)  22.3 us
    unnamed x42, local copies, waits for them, and re-layouts  14.9 us
  transfers between devices with their start and end apart: 9, of which 9 were waited for; matrix products, arithmetic and copies ran while one was open for 11% of the time, Pallas kernels for 0%

profile of v1, /device:TPU:0, one launch (start us, length us, event | category | flops | bytes accessed | tf_op | source)
XLA Modules:
  0.0 409.1 jit_solution(5718477485555910404)
XLA Ops:
  7.2 14.8 %all_gather.15 = bf16[256,512]{1,0:T(8,128)(2,1)S(1)} all-gather(bf16[256,128]{1,0:T(8,128)(2,1)} %bitcast.101), channel_id=1, replica_groups=mesh['kv'=8,'tp'=4] {'tp'}, dimensions={1}, use_global_device_ids=true | all-gather | bytes 327680 | tf_op jit(solution)/shard_map/all_gather | solution.py:83
  22.1 1.6 convolution_convert_fusion.8
  23.8 1.6 convolution_convert_fusion.7
  25.5 2.5 convolution_convert_fusion.3
  28.0 2.5 convolution_convert_fusion.2
  30.6 2.5 convolution_convert_fusion.4
  33.1 0.6 iota_compare_fusion.2
  34.4 0.6 convert_compare_fusion
  35.9 0.6 add_bitcast_fusion
  36.5 12.2 %psum.21 = f32[256]{0:T(256)S(1)} all-reduce(f32[256]{0:T(256)S(1)} %fusion.13), channel_id=1, replica_groups=mesh['kv'=8,'tp'=4] {'kv'}, use_global_device_ids=true, to_apply=%region_4.0 | all-reduce | flops 256 | bytes 2048 | tf_op jit(solution)/shard_map/psum | solution.py:93
  48.7 5.3 %copy.107 = f32[8,128,1024]{1,2,0:T(8,128)} copy(f32[8,128,1024]{2,1,0:T(8,128)} %param.19) | data formatting | bytes 8388608 | tf_op args[2]
  54.1 3.7 reduce-scatter.14.cloned.1.call-done
  57.8 37.1 %reduce-scatter.16.cloned.1.call-done = bf16[32,32]{1,0:T(8,128)(2,1)} async-done(((bf16[256,32]{1,0:T(8,128)(2,1)}), bf16[32,32]{1,0:T(8,128)(2,1)}) %reduce-scatter.16.cloned.1.call-update) | async-done | bytes 2064 | tf_op jit(solution)/shard_map/reduce_scatter | solution.py:105
  94.9 0.8 add_divide_fusion
  95.8 0.7 copy.117
  96.7 35.4 %reduce-scatter.18.cloned.1.call-done = bf16[32,1024]{1,0:T(8,128)(2,1)} async-done(((bf16[256,1024]{1,0:T(8,128)(2,1)}), bf16[32,1024]{1,0:T(8,128)(2,1)}) %reduce-scatter.18.cloned.1.call-update) | async-done | bytes 65552 | tf_op jit(solution)/shard_map/reduce_scatter | solution.py:102
  132.1 37.1 %reduce-scatter.20.cloned.1.call-done = bf16[32,1024]{1,0:T(8,128)(2,1)} async-done(((bf16[256,1024]{1,0:T(8,128)(2,1)}), bf16[32,1024]{1,0:T(8,128)(2,1)}) %reduce-scatter.20.cloned.1.call-update) | async-done | bytes 65552 | tf_op jit(solution)/shard_map/reduce_scatter | solution.py:99
  169.2 37.1 %reduce-scatter.12.cloned.1.call-done = bf16[32,1024]{1,0:T(8,128)(2,1)} async-done(((bf16[256,1024]{1,0:T(8,128)(2,1)}), bf16[32,1024]{1,0:T(8,128)(2,1)}) %reduce-scatter.12.cloned.1.call-update) | async-done | bytes 65552 | tf_op jit(solution)/shard_map/reduce_scatter | solution.py:96
  206.3 1.0 multiply_bitcast_fusion.2
  207.7 0.8 multiply_multiply_fusion.1
  208.7 1.9 fusion.7
  210.5 1.2 fusion.6
  211.8 1.1 slice_reduce_fusion.4
  213.3 0.6 convolution_bitcast_fusion.5
  213.9 0.6 convolution_bitcast_fusion.4
  214.5 8.6 %fusion.2 = f32[8,4,8,128]{3,1,2,0:T(4,128)S(1)} fusion(f32[8,4,8,128]{3,1,2,0:T(4,128)S(1)} %convolution_bitcast_fusion.5, f32[8,4,8,128]{3,1,2,0:T(4,128)S(1)} %convolution_bitcast_fusion.4, f32[8,128,8,128]{1,3,2,0:T(8,128)} %bitcast.87), kind=kOutput, calls=%fused_computation.12 | convolution fusion | flops 50364416 | bytes 4587520 | tf_op jit(solution)/shard_map/nihd,ndhe->nihe/dot_general | solution.py:39
  223.2 0.7 convolution_bitcast_fusion.2
  223.9 6.7 %multiply_reduce_fusion = (f32[8,4,8]{1,2,0:T(8,128)S(1)}, f32[8,4,8,128]{3,1,2,0:T(4,128)S(1)}) fusion(f32[8,4,8,128]{3,1,2,0:T(4,128)S(1)} %convolution_bitcast_fusion.2, f32[8,128,8,128]{1,3,2,0:T(8,128)S(1)} %bitcast.89, f32[8,4,8,128]{3,2,1,0:T(8,128)S(1)} %get-tuple-element.22), kind=kOutput, calls=%fused_computation.46 | convolution fusion | flops 50429696 | bytes 4588544 | tf_op jit(solution)/shard_map/nihd,ndhe->nihe/dot_general | solution.py:41
  231.0 9.8 %all_gather.16 = bf16[256,1024]{1,0:T(8,128)(2,1)S(1)} all-gather(bf16[32,1024]{1,0:T(8,128)(2,1)S(1)} %bitcast.98), channel_id=1, replica_groups=mesh['kv'=8,'tp'=4] {'kv'}, dimensions={0}, use_global_device_ids=true | all-gather | bytes 589824 | tf_op jit(solution)/shard_map/all_gather | solution.py:144
  240.8 2.3 fusion.1
  243.1 1.7 copy.137
  244.9 19.6 %reduce-scatter.22.cloned.1.call-done = bf16[128,112]{1,0:T(8,128)(2,1)} async-done(((bf16[512,112]{1,0:T(8,128)(2,1)}), bf16[128,112]{1,0:T(8,128)(2,1)}) %reduce-scatter.22.cloned.1.call-update) | async-done | bytes 28688
  264.4 0.9 copy.138
  265.3 0.8 fusion.9
  266.1 12.2 %all_gather.17 = bf16[112,512]{1,0:T(8,128)(2,1)S(1)} all-gather(bf16[112,128]{1,0:T(8,128)(2,1)S(1)} %fusion.9), channel_id=1, replica_groups=mesh['kv'=8,'tp'=4] {'tp'}, dimensions={1}, use_global_device_ids=true | all-gather | bytes 143360 | tf_op jit(solution)/shard_map/all_gather | solution.py:154
  278.3 2.5 convolution_convert_fusion
  280.9 3.6 convolution_convert_fusion.1
  284.8 12.6 %psum.23 = f32[112]{0:T(128)S(1)} all-reduce(f32[112]{0:T(128)S(1)} %fusion.15), channel_id=1, replica_groups=mesh['kv'=8,'tp'=4] {'kv'}, use_global_device_ids=true, to_apply=%region_16.17 | all-reduce | flops 112 | bytes 896 | tf_op jit(solution)/shard_map/psum | solution.py:159
  297.4 22.3 %all-gather.3.cloned.1.call-done = bf16[896,2752]{1,0:T(8,128)(2,1)} async-done(((bf16[112,2752]{1,0:T(8,128)(2,1)}), bf16[896,2752]{1,0:T(8,128)(2,1)}) %all-gather.3.cloned.1.call-update) | async-done | bytes 4931600 | tf_op jit(solution)/shard_map/all_gather | solution.py:162
  319.7 4.2 %reduce_sum.62 = bf16[112,2752]{1,0:T(8,128)(2,1)} reduce(bf16[8,112,2752]{2,1,0:T(8,128)(2,1)} %bitcast.91, bf16[]{:T(256)} %constant.56.clone.1), dimensions={0}, to_apply=%region_17.18 | reduce | flops 2157568 | bytes 5548034 | tf_op jit(solution)/shard_map/reduce_sum | solution.py:162
  323.8 54.2 %all-reduce.2.cloned.1.call-done = bf16[112,2752]{1,0:T(8,128)(2,1)} async-done(((bf16[112,2752]{1,0:T(8,128)(2,1)}), bf16[112,2752]{1,0:T(8,128)(2,1)}) %all-reduce.2.cloned.1.call-update) | async-done | bytes 616464 | tf_op jit(solution)/shard_map/psum | solution.py:166
  378.0 2.9 convolution_convert_fusion.6
  380.9 0.7 copy.139
  381.7 10.2 %bitcast_add_fusion = f32[8,128,8,128]{1,3,2,0:T(8,128)} fusion(f32[8,128,8,128]{1,3,2,0:T(8,128)} %bitcast.88, f32[8,4,8,128]{3,1,2,0:T(4,128)S(1)} %fusion.2, f32[8,8]{1,0:T(8,128)S(1)} %fusion.59, f32[8,4,8,128]{3,2,1,0:T(8,128)S(1)} %copy-done.2), kind=kOutput, calls=%fused_computation | convolution fusion | flops 52428800 | bytes 8651008 | tf_op jit(solution)/shard_map/nihd,nihe->ndhe/dot_general | solution.py:46
  391.9 5.4 %copy.133 = f32[8,128,1024]{2,1,0:T(8,128)} copy(f32[8,128,1024]{1,2,0:T(8,128)} %bitcast.90) | data formatting | bytes 8388608
  397.3 3.4 reduce-scatter.24.cloned.1.call-done
  400.7 0.9 copy.140
  401.6 0.9 fusion.8
  (100 shorter events, 3.9 us)
Async XLA Ops:
  7.2 271.2 %copy-start = (bf16[512,2752]{0,1:T(8,128)(2,1)S(1)}, bf16[512,2752]{0,1:T(8,128)(2,1)}, u32[]{:S(2)}) copy-start(bf16[512,2752]{0,1:T(8,128)(2,1)} %param.32) | copy-start | bytes 8454148
  7.2 20.8 %copy-start.6 = (f32[512]{0:T(512)S(1)}, f32[512]{0:T(512)}, u32[]{:S(2)}) copy-start(f32[512]{0:T(512)} %param.20) | copy-start | bytes 6148
  7.2 50.6 %reduce-scatter.14.cloned.1.call-start = ((), (), s32[]{:S(2)}) async-start(), calls=%async_computation.8 | async-start | bytes 73728 | tf_op jit(solution)/shard_map/reduce_scatter | solution.py:108
  23.7 71.2 %reduce-scatter.16.cloned.1.call-start = ((), (), s32[]{:S(2)}) async-start(), calls=%async_computation.9 | async-start | bytes 73728 | tf_op jit(solution)/shard_map/reduce_scatter | solution.py:105
  25.4 106.7 %reduce-scatter.18.cloned.1.call-start = ((), (), s32[]{:S(2)}) async-start(), calls=%async_computation.10 | async-start | bytes 589824 | tf_op jit(solution)/shard_map/reduce_scatter | solution.py:102
  27.9 5.8 %copy-start.11 = (s32[64]{0:T(128)S(1)}, s32[64]{0:T(128)}, u32[]{:S(2)}) copy-start(s32[64]{0:T(128)} %param.18) | copy-start | bytes 772
  27.9 6.2 %copy-start.14 = (f32[32]{0:T(128)S(1)}, f32[32]{0:T(128)}, u32[]{:S(2)}) copy-start(f32[32]{0:T(128)} %param.26) | copy-start | bytes 388
  27.9 6.3 %copy-start.15 = (f32[32]{0:T(128)S(1)}, f32[32]{0:T(128)}, u32[]{:S(2)}) copy-start(f32[32]{0:T(128)} %param.27) | copy-start | bytes 388
  28.0 141.2 %reduce-scatter.20.cloned.1.call-start = ((), (), s32[]{:S(2)}) async-start(), calls=%async_computation.11 | async-start | bytes 589824 | tf_op jit(solution)/shard_map/reduce_scatter | solution.py:99
  30.5 175.8 %reduce-scatter.12.cloned.1.call-start = ((), (), s32[]{:S(2)}) async-start(), calls=%async_computation.7 | async-start | bytes 589824 | tf_op jit(solution)/shard_map/reduce_scatter | solution.py:96
  33.1 231.3 %reduce-scatter.22.cloned.1.call-start = ((), (), s32[]{:S(2)}) async-start(), calls=%async_computation.14 | async-start | bytes 163840
  34.4 19.6 %copy-start.12 = (pred[256]{0:T(512)(128)(4,1)}, pred[256]{0:T(512)(128)(4,1)S(1)}, u32[]{:S(2)}) copy-start(pred[256]{0:T(512)(128)(4,1)S(1)} %lt.76) | copy-start | bytes 772
  206.3 2.4 copy-start.5
  213.3 9.8 %copy-start.3 = (f32[8,4,4,8]{1,2,3,0:T(4,128)S(1)}, f32[8,4,4,8]{1,2,3,0:T(4,128)}, u32[]{:S(2)}) copy-start(f32[8,4,4,8]{1,2,3,0:T(4,128)} %fusion.7) | copy-start | bytes 12292
  213.3 10.6 %copy-start.1 = (f32[8,128,1024]{1,2,0:T(8,128)S(1)}, f32[8,128,1024]{1,2,0:T(8,128)}, u32[]{:S(2)}) copy-start(f32[8,128,1024]{1,2,0:T(8,128)} %copy.107) | copy-start | bytes 12582916
  223.9 7.0 %copy-start.9 = (f32[128]{0:T(128)S(1)}, f32[128]{0:T(128)}, u32[]{:S(2)}) copy-start(f32[128]{0:T(128)} %param.28) | copy-start | bytes 1540
  230.6 34.7 %copy-start.4 = (bf16[64,4,128]{2,1,0:T(4,128)(2,1)S(1)}, bf16[64,4,128]{2,1,0:T(4,128)(2,1)}, u32[]{:S(2)}) copy-start(bf16[64,4,128]{2,1,0:T(4,128)(2,1)} %param.17) | copy-start | bytes 196612
  243.1 37.8 %copy-start.7 = (f32[512]{0:T(512)S(1)}, f32[512]{0:T(512)}, u32[]{:S(2)}) copy-start(f32[512]{0:T(512)} %param.30) | copy-start | bytes 6148
  244.8 74.9 %all-gather.3.cloned.1.call-start = ((), (), s32[]{:S(2)}) async-start(), calls=%async_computation.13 | async-start | bytes 5677056 | tf_op jit(solution)/shard_map/all_gather | solution.py:162
  280.9 97.1 %all-reduce.2.cloned.1.call-start = ((), (), s32[]{:S(2)}) async-start(), calls=%async_computation.12 | async-start | bytes 1261568 | tf_op jit(solution)/shard_map/psum | solution.py:166
  284.6 116.1 %reduce-scatter.24.cloned.1.call-start = ((), (), s32[]{:S(2)}) async-start(), calls=%async_computation.15 | async-start | bytes 163840
  323.8 57.8 %copy-start.2 = (f32[8,4,8,128]{3,2,1,0:T(8,128)S(1)}, f32[8,4,8,128]{3,2,1,0:T(8,128)}, u32[]{:S(2)}) copy-start(f32[8,4,8,128]{3,2,1,0:T(8,128)} %get-tuple-element.42) | copy-start | bytes 393220
  391.9 9.7 %copy-start.8 = (s32[256]{0:T(256)S(1)}, s32[256]{0:T(256)}, u32[]{:S(2)}) copy-start(s32[256]{0:T(256)} %add_bitcast_fusion) | copy-start | bytes 3076
  391.9 9.7 %copy-start.10 = (pred[256]{0:T(512)(128)(4,1)S(1)}, pred[256]{0:T(512)(128)(4,1)}, u32[]{:S(2)}) copy-start(pred[256]{0:T(512)(128)(4,1)} %convert_compare_fusion) | copy-start | bytes 772
  391.9 9.7 %copy-start.13 = (pred[256]{0:T(512)(128)(4,1)S(1)}, pred[256]{0:T(512)(128)(4,1)}, u32[]{:S(2)}) copy-start(pred[256]{0:T(512)(128)(4,1)} %copy-done.12) | copy-start | bytes 772
Sparse Core Ops, SparseCore 0:
  23.8 33.8 reduce-scatter.13
  61.3 33.4 reduce-scatter.15
  97.9 34.1 reduce-scatter.17
  135.0 34.1 reduce-scatter.19
  172.1 34.1 reduce-scatter.11
  244.9 19.4 reduce-scatter.21
  281.0 38.6 all-gather.2
  322.8 55.1 all-reduce.1
  381.8 18.9 reduce-scatter.23
